TPU v7x, 32 devices: a whole 2x2x4 slice. The times are simulated.
32 devices in a mesh: kv: 8 (over z, y), tp: 4 (over x, core).
Axes of the slice: x: 2, y: 2, z: 4, core: 2. Of those that a mesh axis runs over, the one named last changes fastest.
Arguments:
- queries: bfloat16 [2, 3072, 1024], P(None, 'kv', 'tp'), may hold values from -112 to 112
- key_states: bfloat16 [2, 3072, 256], P(None, 'kv', 'tp'), may hold values from -4 to 4
- value_states: bfloat16 [2, 3072, 256], P(None, 'kv', 'tp'), may hold values from -6 to 6
- cotangent: bfloat16 [2, 3072, 1024], P(None, 'kv', 'tp'), may hold values from -6 to 6
- gate_logits: float32 [2, 3072, 16], P(None, 'kv', 'tp'), may hold values from -6 to 6
- layer_input: bfloat16 [2, 3072, 4096], P(None, ('kv', 'tp')), may hold values from -6 to 6
- chosen: int32 [2, 48, 4, 16], P(None, 'kv', 'tp'), may hold values from 0 to 47, as said below
Outputs:
- query_grad: bfloat16 [2, 3072, 1024], P(None, 'kv', 'tp')
- key_grad: bfloat16 [2, 3072, 256], P(None, 'kv', 'tp')
- value_grad: bfloat16 [2, 3072, 256], P(None, 'kv', 'tp')
- value_weight_grad: float32 [4096, 256], P(('kv', 'tp'))
Inputs may be any that keep to these rules, and one draw needn't show every extreme that they name: `chosen`: for each sequence, query block b and key head, the 16 entries are distinct blocks; they include b itself and block 0; blocks after b hold only keys after all of the block's queries. Taking the 6 query blocks of one index of kv together (aligned), one sequence and one key head, at most 2 distinct blocks held by any one earlier index of kv are named, and some index reaches 2.
All inputs are finite; a program needn't handle non-finite values.
Results may differ from a plain program's by a relative error of at most 0.0058.
Values may be sent and summed in bfloat16 or wider, within the bound.
No kernel may reach another device: no remote copies, remote signals or barrier semaphores. Data moves between devices by JAX's collectives and lax.ppermute only.
A program may use at most 128 MiB of HBM per device.

v0:
```python
import functools
import math

import jax
import jax.numpy as jnp
from jax import lax
from jax.experimental import pallas as pl
from jax.experimental.pallas import tpu as pltpu
from jax.sharding import PartitionSpec as P


BLK = 64
MOST = 2
LABEL_ROWS = 16
CUTS = 4
LOG2E = math.log2(math.e)
KV = ("hi", "lo")
BF = jnp.bfloat16
F32 = jnp.float32
VMEM = pltpu.VMEM
SMEM = pltpu.SMEM
MIB = 1024 * 1024


def grant(mib):
    return pltpu.CompilerParams(vmem_limit_bytes=mib * MIB)


def vspec():
    return pl.BlockSpec(memory_space=VMEM)


def sspec():
    return pl.BlockSpec(memory_space=SMEM)


def prep_kernel(
    n, bpd, heads, hd, scale, ids, table, own_ref, q_ref, g_ref, gate_ref, r_ref, kv_loc, acc_loc
):
    width = 2 * hd
    rows = heads * BLK
    low = lax.broadcasted_iota(jnp.int32, (BLK, width), 1) < hd

    def step(i, carry):
        at = pl.ds(pl.multiple_of(i * BLK, BLK), BLK)
        gates = jax.nn.sigmoid(gate_ref[at, :])
        for pair in range(heads // 2):
            q = q_ref[at, pair * width : (pair + 1) * width].astype(F32) * scale
            g = g_ref[at, pair * width : (pair + 1) * width].astype(F32)
            gv = jnp.where(low, gates[:, 2 * pair : 2 * pair + 1], gates[:, 2 * pair + 1 : 2 * pair + 2])
            g = g * gv
            qr = pltpu.roll(q, hd, 1)
            gr = pltpu.roll(g, hd, 1)
            zero = jnp.zeros_like(q)
            base = 2 * pair * BLK
            r_ref[i, base : base + BLK, :] = jnp.where(low, q, zero).astype(BF)
            r_ref[i, base + BLK : base + 2 * BLK, :] = jnp.where(low, qr, zero).astype(BF)
            r_ref[i, rows + base : rows + base + BLK, :] = jnp.where(low, zero, gr).astype(BF)
            r_ref[i, rows + base + BLK : rows + base + 2 * BLK, :] = jnp.where(low, zero, g).astype(BF)
        return carry

    nblk = q_ref.shape[0] // BLK
    lax.fori_loop(0, nblk, step, 0)

    seqs = nblk // bpd
    own = own_ref[0]
    dummy = nblk + n * seqs * MOST
    named = ids[...]
    row = lax.broadcasted_iota(jnp.int32, named.shape, 0)
    start = lax.broadcasted_iota(jnp.int32, named.shape, 1) == 0
    s = jnp.zeros_like(row)
    for k in range(1, seqs):
        s = s + (row >= k * bpd).astype(jnp.int32)
    block = own * bpd + row - s * bpd
    c = jnp.where(start, block, jnp.where(named == block, named[:, 0:1], named))
    h = lax.shift_right_logical(c * -(-(1 << 20) // bpd), 20)
    w = c - h * bpd
    low = jnp.zeros_like(c)
    for k in range(n):
        here = jnp.full_like(c, table[k * seqs])
        for q in range(1, seqs):
            here = jnp.where(s == q, table[k * seqs + q], here)
        low = jnp.where(h == k, here, low)
    slot = (w != low).astype(jnp.int32)
    own_z = lax.shift_right_logical(own, 1)
    h_z = lax.shift_right_logical(h, 1)
    home = s * bpd + w
    far = 2 * nblk + (((own_z - h_z - 1) * seqs + s) * 2 + (h & 1)) * MOST + slot
    near = jnp.where(h == own, home, nblk + home)
    future = c > block
    kv_loc[...] = jnp.where(future, 0, jnp.where(h_z == own_z, near, far))
    remote = nblk + (h * seqs + s) * MOST + slot
    acc_loc[...] = jnp.where(future, dummy, jnp.where(h == own, home, remote))


def pack_kernel(seqs, bpd, n, shifts, *refs):
    tables = refs[:shifts]
    own_ref, kv_ref, partner_ref = refs[shifts : shifts + 3]
    outs = refs[shifts + 3 : 2 * shifts + 3]
    both = refs[2 * shifts + 3]
    rows = kv_ref.shape[0]
    both[0:rows, :] = kv_ref[...]
    both[rows : 2 * rows, :] = partner_ref[...]
    own = own_ref[0]
    side = own & 1
    for d in range(shifts):
        for s in range(seqs):
            for yh in range(2):
                for m in range(MOST):
                    slot = (s * 2 + yh) * MOST + m
                    lab = tables[d][m * n * seqs + (own - side + yh) * seqs + s]
                    at = ((side ^ yh) * seqs + s) * bpd + lab
                    src = pl.multiple_of(at * BLK, BLK)
                    outs[d][slot * BLK : (slot + 1) * BLK, :] = both[pl.ds(src, BLK), :]


def attend_kernel(
    n,
    nblk,
    bpd,
    heads,
    hd,
    picks,
    scale,
    kv_loc,
    acc_loc,
    table,
    r_ref,
    kv_ref,
    partner_ref,
    *refs,
):
    zshifts = n // 2 - 1
    far = refs[:zshifts]
    dq_ref, own_ref, out_ref, kv_all, acc, dq_buf = refs[zshifts : zshifts + 6]
    sets = refs[zshifts + 6 :]
    kv_picks, s_bufs, p_bufs, x_bufs = sets[0:2], sets[2:4], sets[4:6], sets[6:8]
    rows = heads * BLK
    width = 2 * hd
    seqs = nblk // bpd
    slots = seqs * MOST
    dummy = nblk + n * slots
    chunk = 4 * BLK
    keys = picks * BLK

    pair_rows = 2 * nblk * BLK
    kv_all[0 : nblk * BLK, :] = kv_ref[...]
    kv_all[nblk * BLK : pair_rows, :] = partner_ref[...]
    for d in range(zshifts):
        span = far[d].shape[0]
        kv_all[pair_rows + d * span : pair_rows + (d + 1) * span, :] = far[d][...]
    acc[...] = jnp.zeros_like(acc)
    x_bufs[1][...] = jnp.zeros_like(x_bufs[1])
    kv_picks[1][...] = jnp.zeros_like(kv_picks[1])
    kpos = lax.broadcasted_iota(jnp.int32, (BLK, rows), 0)
    qpos = lax.broadcasted_iota(jnp.int32, (BLK, rows), 1) % BLK
    diag = kpos <= qpos

    def fold(x, op):
        out = x[0:8, :]
        for i in range(1, x.shape[0] // 8):
            out = op(out, x[i * 8 : (i + 1) * 8, :])
        return out

    def gather(i, side):
        for j in range(picks):
            src = pl.multiple_of(kv_loc[i, j] * BLK, BLK)
            kv_picks[side][j * BLK : (j + 1) * BLK, :] = kv_all[pl.ds(src, BLK), :]

    def score(i, side):
        kv_pick, s_buf, p_buf = kv_picks[side], s_bufs[side], p_bufs[side]
        r = r_ref[i]
        for c in range(keys // chunk):
            both = lax.dot_general(
                kv_pick[c * chunk : (c + 1) * chunk, :], r, (((1,), (1,)), ((), ())), preferred_element_type=F32
            )
            p_buf[c * chunk : (c + 1) * chunk, :] = both[:, rows:]
            for j in range(4):
                pick = c * 4 + j
                s = both[j * BLK : (j + 1) * BLK, :rows] * LOG2E
                if pick == 0:
                    s = jnp.where(diag, s, -jnp.inf)
                else:
                    bias = jnp.where(acc_loc[i, pick] == dummy, -jnp.inf, 0.0).astype(F32)
                    s = s + bias
                s_buf[pick * BLK : (pick + 1) * BLK, :] = s
            yield

    def weigh(side):
        s_buf, p_buf, x_buf = s_bufs[side], p_bufs[side], x_bufs[side]
        top = jnp.full((8, rows), -jnp.inf, F32)
        for j in range(picks):
            top = jnp.maximum(top, fold(s_buf[j * BLK : (j + 1) * BLK, :], jnp.maximum))
            yield 1
        top = jnp.max(top, axis=0, keepdims=True)
        total = jnp.zeros((8, rows), F32)
        for j in range(picks):
            e = jnp.exp2(s_buf[j * BLK : (j + 1) * BLK, :] - top)
            total = total + fold(e, jnp.add)
            yield 3
        shift = top + jnp.log2(jnp.sum(total, axis=0, keepdims=True))
        dot = jnp.zeros((8, rows), F32)
        for j in range(picks):
            at = slice(j * BLK, (j + 1) * BLK)
            w = jnp.exp2(s_buf[at, :] - shift)
            wb = w.astype(BF)
            s_buf[at, :] = w
            x_buf[at, rows:] = wb
            dot = dot + fold(wb.astype(F32) * p_buf[at, :], jnp.add)
            yield 6
        dot = jnp.sum(dot, axis=0, keepdims=True)
        for j in range(picks):
            at = slice(j * BLK, (j + 1) * BLK)
            x_buf[at, :rows] = (s_buf[at, :] * (p_buf[at, :] - dot)).astype(BF)
            yield 3

    def spread(i, side):
        kv_pick, x_buf = kv_picks[side], x_bufs[side]
        r = r_ref[i]
        dqt = jnp.zeros((width, rows), F32)
        for c in range(keys // chunk):
            at = slice(c * chunk, (c + 1) * chunk)
            x = x_buf[at, :]
            grads = lax.dot_general(x, r, (((1,), (0,)), ((), ())), preferred_element_type=F32)
            for j in range(4):
                dst = pl.multiple_of(acc_loc[i, c * 4 + j] * BLK, BLK)
                acc[pl.ds(dst, BLK), :] += grads[j * BLK : (j + 1) * BLK, :]
            dqt = dqt + lax.dot_general(
                kv_pick[at, :], x[:, :rows], (((0,), (0,)), ((), ())), preferred_element_type=F32
            )
            yield
        dq_buf[...] = dqt[:hd, :] * scale
        row_at = pl.ds(pl.multiple_of(i * BLK, BLK), BLK)
        for pair in range(heads // 2):
            two = jnp.concatenate(
                [dq_buf[:, 2 * pair * BLK : (2 * pair + 1) * BLK], dq_buf[:, (2 * pair + 1) * BLK : (2 * pair + 2) * BLK]],
                axis=0,
            )
            dq_ref[row_at, pair * width : (pair + 1) * width] = two.T.astype(BF)
        yield

    def drain(steps):
        for _ in steps:
            pass

    def turn(i, side):
        other = 1 - side
        after = jnp.minimum(i + 1, nblk - 1)

        def matmuls():
            yield from spread(jnp.maximum(i - 1, 0), other)
            gather(after, other)
            yield from score(after, other)

        pending = matmuls()
        parts = 2 * (keys // chunk) + 1
        whole = 13 * picks
        done = taken = 0
        for units in weigh(side):
            done += units
            while taken < parts and done * parts >= (taken + 1) * whole * 0.9:
                next(pending)
                taken += 1
        drain(pending)

    gather(0, 0)
    drain(score(0, 0))

    def step(i, carry):
        @pl.when(i % 2 == 0)
        def _():
            turn(i, 0)

        @pl.when(i % 2 == 1)
        def _():
            turn(i, 1)

        return carry

    lax.fori_loop(0, nblk, step, 0)
    drain(spread(nblk - 1, 1))
    own_ref[...] = acc[0 : nblk * BLK, :]
    lane = lax.broadcasted_iota(jnp.int32, (LABEL_ROWS, width), 0)
    for h in range(n):
        lo = (nblk + h * slots) * BLK
        out_ref[h, 0 : slots * BLK, :] = acc[lo : lo + slots * BLK, :].astype(BF)
        mark = jnp.zeros((LABEL_ROWS, width), F32)
        for k in range(slots):
            lab = table[(k % MOST) * n * seqs + h * seqs + k // MOST]
            mark = jnp.where(lane == k, lab.astype(F32), mark)
        out_ref[h, slots * BLK : slots * BLK + LABEL_ROWS, :] = mark.astype(BF)


def combine_kernel(n, seqs, bpd, hd, parts, quarter, own_ref, msgs, *refs):
    sources = refs[:parts]
    kg_ref, vg_ref, out_ref, total, vbuf, pieces, sems = refs[parts:]
    cut = sources[0].shape[0] // CUTS
    copies = [
        pltpu.make_async_copy(
            sources[j].at[pl.ds(q * cut, cut)], pieces.at[j, pl.ds(q * cut, cut)], sems.at[j, q]
        )
        for q in range(CUTS)
        for j in range(parts)
    ]
    for copy in copies:
        copy.start()
    slots = seqs * MOST
    total[...] = own_ref[...]
    for d in range(n):
        marks = msgs[d, slots * BLK : slots * BLK + LABEL_ROWS, :].astype(F32)
        for s in range(seqs):
            for m in range(MOST):
                k = s * MOST + m
                val = msgs[d, k * BLK : (k + 1) * BLK, :].astype(F32)
                mark = marks[k : k + 1, :]
                for b in range(bpd):
                    at = slice((s * bpd + b) * BLK, (s * bpd + b + 1) * BLK)
                    total[at, :] = total[at, :] + jnp.where(mark == float(b), val, 0.0)
    tok = bpd * BLK
    kg_ref[...] = total[:, :hd].astype(BF)
    vg = total[:, hd:].astype(BF)
    vg_ref[...] = vg
    vbuf[...] = vg
    span = tok // parts
    turned = []
    for j in range(parts):
        who = jnp.bitwise_xor(quarter[0], j)
        v = [
            vbuf[pl.ds(pl.multiple_of(s * tok + who * span, 16), span), :].astype(F32)
            for s in range(seqs)
        ]
        turned.append(jnp.concatenate(v, axis=0).T.astype(BF))
    lanes = out_ref.shape[2]
    for copy in copies:
        copy.wait()
    for i in range(out_ref.shape[0] // 2):
        acc = jnp.zeros((hd, 2 * lanes), F32)
        for j in range(parts):
            x = pieces[j, :, 2 * i * lanes : 2 * (i + 1) * lanes]
            acc = acc + jnp.dot(turned[j], x, preferred_element_type=F32)
        out_ref[2 * i] = acc[:, :lanes].astype(BF)
        out_ref[2 * i + 1] = acc[:, lanes:].astype(BF)


def final_kernel(n, parts, in_ref, out_ref):
    for t in range(parts):
        acc = in_ref[t].astype(F32)
        for k in range(1, n):
            acc = acc + in_ref[k * parts + t].astype(F32)
        if t % 2 == 0:
            held = acc
        else:
            both = jnp.concatenate([held, acc], axis=0)
            w = both.shape[0]
            out_ref[:, (t // 2) * w : (t // 2 + 1) * w] = both.T


def on_device(queries, key_states, value_states, cotangent, gate_logits, layer_input, chosen):
    seqs, tok, row_width = queries.shape
    hd = key_states.shape[2]
    heads = row_width // hd
    bpd = tok // BLK
    picks = chosen.shape[3]
    pairs = lax.axis_size("hi")
    n = 2 * pairs
    parts = lax.axis_size("tp")
    own = lax.axis_index(KV).astype(jnp.int32)
    t_own = lax.axis_index("tp").astype(jnp.int32)
    scale = hd ** (-0.5)
    assert math.log2(scale).is_integer() and n % 2 == 0
    nblk = seqs * bpd
    slots = seqs * MOST
    zshifts = pairs - 1
    width = 2 * hd

    perm = lax.ppermute
    kv = jnp.concatenate([key_states, value_states], axis=-1).reshape(nblk * BLK, width)
    partner = perm(kv, "lo", [(0, 1), (1, 0)])

    kv, chosen = lax.optimization_barrier((kv, chosen))
    ids = chosen[:, :, 0, :]
    flat = ids.reshape(seqs, bpd * picks)
    holder = (flat // bpd)[None]
    within = (flat % bpd)[None]
    hit = holder == jnp.arange(n, dtype=jnp.int32)[:, None, None]
    low = jnp.min(jnp.where(hit, within, bpd - 1), axis=-1)
    high = jnp.max(jnp.where(hit, within, 0), axis=-1)
    table = jnp.stack([low, high]).reshape(MOST * n * seqs)
    own_at = own.reshape(1)
    asked = [
        perm(table, "hi", [(k, k - d) for k in range(d, pairs)]) for d in range(1, pairs)
    ]

    tp_xor = lambda j: [(i, i ^ j) for i in range(parts)]
    mine = layer_input.reshape(seqs * layer_input.shape[1], layer_input.shape[2])
    piece2 = perm(mine, "tp", tp_xor(2))
    piece1 = perm(mine, "tp", tp_xor(1))

    prepare = pl.pallas_call(
        functools.partial(prep_kernel, n, bpd, heads, hd, scale),
        out_shape=[
            jax.ShapeDtypeStruct((nblk, 2 * heads * BLK, width), BF),
            jax.ShapeDtypeStruct((nblk, picks), jnp.int32),
            jax.ShapeDtypeStruct((nblk, picks), jnp.int32),
        ],
        in_specs=[vspec()] + [sspec()] * 2 + [vspec()] * 3,
        out_specs=[vspec()] * 3,
        compiler_params=grant(3),
        name="prep",
    )
    r, kv_loc, acc_loc = prepare(
        ids.reshape(nblk, picks),
        table,
        own_at,
        queries.reshape(seqs * tok, row_width),
        cotangent.reshape(seqs * tok, row_width),
        gate_logits.reshape(seqs * tok, heads),
    )

    zrows = slots * 2 * BLK
    packed = pl.pallas_call(
        functools.partial(pack_kernel, seqs, bpd, n, zshifts),
        out_shape=[jax.ShapeDtypeStruct((zrows, width), BF)] * zshifts,
        in_specs=[sspec()] * (zshifts + 1) + [vspec()] * 2,
        out_specs=[vspec()] * zshifts,
        scratch_shapes=[VMEM((2 * nblk * BLK, width), BF)],
        compiler_params=grant(3),
        name="pack",
    )(*asked, own_at, kv, partner)
    far = [
        perm(packed[d - 1], "hi", [(k, k + d) for k in range(pairs - d)]) for d in range(1, pairs)
    ]
    dummy = nblk + n * slots

    keys = picks * BLK
    rows = heads * BLK
    mrows = slots * BLK + LABEL_ROWS
    attended = pl.pallas_call(
        functools.partial(attend_kernel, n, nblk, bpd, heads, hd, picks, scale),
        out_shape=[
            jax.ShapeDtypeStruct((seqs * tok, row_width), BF),
            jax.ShapeDtypeStruct((nblk * BLK, width), F32),
            jax.ShapeDtypeStruct((n, mrows, width), BF),
        ],
        in_specs=[sspec()] * 3 + [vspec()] * (3 + zshifts),
        out_specs=[vspec()] * 3,
        scratch_shapes=[
            VMEM((2 * nblk * BLK + zshifts * zrows, width), BF),
            VMEM(((dummy + 1) * BLK, width), F32),
            VMEM((hd, rows), F32),
        ]
        + [VMEM((keys, width), BF)] * 2
        + [VMEM((keys, rows), F32)] * 4
        + [VMEM((keys, 2 * rows), BF)] * 2,
        compiler_params=grant(14),
        name="attend",
    )(kv_loc, acc_loc, table, r, kv, partner, *far)
    query_grad = attended[0].reshape(seqs, tok, row_width)
    arrived = lax.all_to_all(attended[2], KV, split_axis=0, concat_axis=0, tiled=True)
    own_sum, piece2 = lax.optimization_barrier((attended[1], piece2))
    piece3 = perm(piece2, "tp", tp_xor(1))
    pieces = [mine, piece1, piece2, piece3]

    ranks = n * parts
    depth = layer_input.shape[2]
    share = depth // ranks
    kg, vg, partial = pl.pallas_call(
        functools.partial(combine_kernel, n, seqs, bpd, hd, parts),
        out_shape=[
            jax.ShapeDtypeStruct((seqs * tok, hd), BF),
            jax.ShapeDtypeStruct((seqs * tok, hd), BF),
            jax.ShapeDtypeStruct((ranks * share // 128, hd, 128), BF),
        ],
        in_specs=[sspec()] + [vspec()] * 2 + [pl.BlockSpec(memory_space=pl.ANY)] * parts,
        out_specs=[vspec()] * 3,
        scratch_shapes=[
            VMEM((nblk * BLK, width), F32),
            VMEM((seqs * tok, hd), BF),
            VMEM((parts,) + mine.shape, BF),
            pltpu.SemaphoreType.DMA((parts, CUTS)),
        ],
        compiler_params=grant(10),
        name="combine",
    )(t_own.reshape(1), own_sum, arrived, *pieces)
    key_grad = kg.reshape(seqs, tok, hd)
    value_grad = vg.reshape(seqs, tok, hd)
    if share != 128:
        partial = partial.transpose(1, 0, 2).reshape(hd, ranks, share).transpose(1, 0, 2)
    swapped = lax.all_to_all(partial, KV + ("tp",), split_axis=0, concat_axis=0, tiled=True)
    value_weight_grad = pl.pallas_call(
        functools.partial(final_kernel, n, parts),
        out_shape=jax.ShapeDtypeStruct((share, parts * hd), F32),
        in_specs=[vspec()],
        out_specs=vspec(),
        compiler_params=grant(2),
        name="final",
    )(swapped)
    return query_grad, key_grad, value_grad, value_weight_grad


def solution(mesh):
    count = mesh.shape["kv"]
    split = jax.sharding.Mesh(
        mesh.devices.reshape(count // 2, 2, mesh.shape["tp"]), ("hi", "lo", "tp")
    )
    in_specs = (
        P(None, KV, "tp"),
        P(None, KV, "tp"),
        P(None, KV, "tp"),
        P(None, KV, "tp"),
        P(None, KV, "tp"),
        P(None, KV + ("tp",), None),
        P(None, KV, "tp", None),
    )
    out_specs = (
        P(None, KV, "tp"),
        P(None, KV, "tp"),
        P(None, KV, "tp"),
        P(KV + ("tp",), None),
    )

    return jax.shard_map(
        on_device, mesh=split, in_specs=in_specs, out_specs=out_specs, check_vma=False
    )
```

profile of v0, /device:TPU:0, one launch (start us, length us, event | category | flops | bytes accessed | tf_op | source)
XLA Modules:
  0.0 91.4 jit_solution(2645968728937445784)
XLA Ops:
  0.7 3.0 %collective-permute-start.7 = (bf16[192,4096]{1,0:T(8,128)(2,1)}, bf16[192,4096]{1,0:T(8,128)(2,1)}, u32[]{:S(2)}, u32[]{:S(2)}) collective-permute-start(bf16[192,4096]{1,0:T(8,128)(2,1)} %bitcast.15), channel_id=1, source_target_pairs={{0,2},{1,3},{2,0},{3,1},{4,6},{5,7},{6,4},{7,5},{8,10},{9,11},{10,... | collective-permute-start | bytes 4718600 | tf_op jit(solution)/shard_map/ppermute | solution.py:396
  3.7 1.0 %pad_maximum_fusion = bf16[2,384,128]{1,2,0:T(8,128)(2,1)S(1)} fusion(bf16[2,384,64]{1,2,0:T(8,128)(2,1)} %param.9, bf16[2,384,64]{1,2,0:T(8,128)(2,1)} %param.8), kind=kLoop, calls=%fused_computation | loop fusion | flops 393216 | bytes 393216 | tf_op jit(solution)/shard_map/concatenate | solution.py:377
  4.6 0.2 copy.21
  4.8 1.6 %collective-permute-start = (bf16[768,128]{1,0:T(8,128)(2,1)S(1)}, bf16[768,128]{1,0:T(8,128)(2,1)S(1)}, u32[]{:S(2)}, u32[]{:S(2)}) collective-permute-start(bf16[768,128]{1,0:T(8,128)(2,1)S(1)} %bitcast.12), channel_id=1, source_target_pairs={{0,4},{4,0},{1,5},{5,1},{2,6},{6,2},{3,7},{7,3},{8,12},{12,8},{9,1... | collective-permute-start | bytes 589832 | tf_op jit(solution)/shard_map/ppermute | solution.py:378
  6.4 0.7 compare_reduce_fusion
  7.1 0.1 ne.42
  7.2 0.8 divide_reduce_fusion
  8.2 0.2 select_reduce_fusion.1
  8.3 0.1 copy.22
  8.4 0.1 reshape.74.table
  8.5 1.3 %collective-permute-start.3 = (s32[32]{0:T(128)S(1)}, s32[32]{0:T(128)S(1)}, u32[]{:S(2)}, u32[]{:S(2)}) collective-permute-start(s32[32]{0:T(128)S(1)} %reshape.74.table), channel_id=1, source_target_pairs={{24,0},{25,1},{26,2},{27,3},{28,4},{29,5},{30,6},{31,7}} | collective-permute-start | bytes 392 | tf_op jit(solution)/shard_map/ppermute | solution.py:391
  9.8 1.3 %collective-permute-start.2 = (s32[32]{0:T(128)S(1)}, s32[32]{0:T(128)S(1)}, u32[]{:S(2)}, u32[]{:S(2)}) collective-permute-start(s32[32]{0:T(128)S(1)} %reshape.74.table), channel_id=1, source_target_pairs={{16,0},{24,8},{17,1},{25,9},{18,2},{26,10},{19,3},{27,11},{20,4},{... | collective-permute-start | bytes 392 | tf_op jit(solution)/shard_map/ppermute | solution.py:391
  11.1 1.3 %collective-permute-start.1 = (s32[32]{0:T(128)S(1)}, s32[32]{0:T(128)S(1)}, u32[]{:S(2)}, u32[]{:S(2)}) collective-permute-start(s32[32]{0:T(128)S(1)} %reshape.74.table), channel_id=1, source_target_pairs={{8,0},{16,8},{24,16},{9,1},{17,9},{25,17},{10,2},{18,10},{26,18},{... | collective-permute-start | bytes 392 | tf_op jit(solution)/shard_map/ppermute | solution.py:391
  12.4 3.4 %collective-permute-done.3.refs_2_ = s32[32]{0:T(128)S(1)} collective-permute-done((s32[32]{0:T(128)S(1)}, s32[32]{0:T(128)S(1)}, u32[]{:S(2)}, u32[]{:S(2)}) %collective-permute-start.3) | collective-permute-done | bytes 160 | tf_op jit(solution)/shard_map/ppermute | solution.py:391
  15.8 0.4 collective-permute-done.2.refs_1_
  16.2 0.4 collective-permute-done.1.refs_0_
  16.6 0.6 pack.1
  17.2 4.0 %collective-permute-start.4 = (bf16[512,128]{1,0:T(8,128)(2,1)S(1)}, bf16[512,128]{1,0:T(8,128)(2,1)S(1)}, u32[]{:S(2)}, u32[]{:S(2)}) collective-permute-start(bf16[512,128]{1,0:T(8,128)(2,1)S(1)} %get-tuple-element.25), channel_id=1, source_target_pairs={{0,8},{8,16},{16,24},{1,9},{9,17},{17,25},{2,10},{10,18},{18,26},{... | collective-permute-start | bytes 393224 | tf_op jit(solution)/shard_map/ppermute | solution.py:431
  21.2 3.4 %collective-permute-start.5 = (bf16[512,128]{1,0:T(8,128)(2,1)S(1)}, bf16[512,128]{1,0:T(8,128)(2,1)S(1)}, u32[]{:S(2)}, u32[]{:S(2)}) collective-permute-start(bf16[512,128]{1,0:T(8,128)(2,1)S(1)} %get-tuple-element.26), channel_id=1, source_target_pairs={{0,16},{8,24},{1,17},{9,25},{2,18},{10,26},{3,19},{11,27},{4,20},{... | collective-permute-start | bytes 393224 | tf_op jit(solution)/shard_map/ppermute | solution.py:431
  24.6 1.3 %collective-permute-start.6 = (bf16[512,128]{1,0:T(8,128)(2,1)S(1)}, bf16[512,128]{1,0:T(8,128)(2,1)S(1)}, u32[]{:S(2)}, u32[]{:S(2)}) collective-permute-start(bf16[512,128]{1,0:T(8,128)(2,1)S(1)} %get-tuple-element.27), channel_id=1, source_target_pairs={{0,24},{1,25},{2,26},{3,27},{4,28},{5,29},{6,30},{7,31}} | collective-permute-start | bytes 393224 | tf_op jit(solution)/shard_map/ppermute | solution.py:431
  26.0 0.9 copy.23
  26.9 2.8 %prep.1 = (bf16[12,512,128]{2,1,0:T(8,128)(2,1)S(1)}, s32[12,16]{1,0:T(8,128)S(1)}, s32[12,16]{1,0:T(8,128)S(1)}) custom-call(s32[12,16]{1,0:T(8,128)S(1)} %reshape_squeeze.4.ids, s32[32]{0:T(128)S(1)} %reshape.74.table, s32[1]{0:T(128)} %bitcast.3.own_ref.refs_3_, bf16[768,256]{1,0:T(8,128)(2,1)S(1)} %bitcast.19, bf16[768,256]{1,0:T(8,128)(2,1)S(1)} %bitcast.20, ...), custom_call_target="tpu_custom_call" | custom-call | tf_op jit(solution)/shard_map/prep/pallas_call | solution.py:411
  29.7 14.4 %attend.1 = (bf16[768,256]{1,0:T(8,128)(2,1)}, f32[768,128]{1,0:T(8,128)S(1)}, bf16[8,272,128]{2,1,0:T(8,128)(2,1)}) custom-call(s32[12,16]{1,0:T(8,128)S(1)} %get-tuple-element.21.kv_loc, s32[12,16]{1,0:T(8,128)S(1)} %get-tuple-element.22.acc_loc, s32[32]{0:T(128)S(1)} %reshape.74.table, bf16[12,512,128]{2,1,0:T(8,128)(2,1)S(1)} %get-tuple-element.23.r_ref, ...), custom_call_target="tpu_custom_call" | custom-call | tf_op jit(solution)/shard_map/attend/pallas_call | solution.py:438
  44.1 0.5 collective-permute-start.9
  44.6 6.7 %all-to-all-start = ((bf16[8,272,128]{2,1,0:T(8,128)(2,1)}), bf16[8,272,128]{2,1,0:T(8,128)(2,1)S(1)}, u32[]{:S(2)}, u32[]{:S(2)}) async-start(bf16[8,272,128]{2,1,0:T(8,128)(2,1)} %get-tuple-element.31), calls=%async_computation | async-start | bytes 1114112 | tf_op jit(solution)/shard_map/all_to_all | solution.py:459
  51.3 15.8 %all-to-all-done.msgs = bf16[8,272,128]{2,1,0:T(8,128)(2,1)S(1)} async-done(((bf16[8,272,128]{2,1,0:T(8,128)(2,1)}), bf16[8,272,128]{2,1,0:T(8,128)(2,1)S(1)}, u32[]{:S(2)}, u32[]{:S(2)}) %all-to-all-start) | async-done | bytes 557088 | tf_op jit(solution)/shard_map/all_to_all | solution.py:459
  67.2 5.0 %combine.1 = (bf16[768,64]{1,0:T(8,128)(2,1)S(1)}, bf16[768,64]{1,0:T(8,128)(2,1)S(1)}, bf16[32,64,128]{2,1,0:T(8,128)(2,1)}) custom-call(s32[1]{0:T(128)} %bitcast.8.quarter, f32[768,128]{1,0:T(8,128)S(1)} %get-tuple-element.30.own_ref, bf16[8,272,128]{2,1,0:T(8,128)(2,1)S(1)} %all-to-all-done.msgs, bf16[192,4096]{1,0:T(8,128)(2,1)S(1)} %bitcast.17, ...), custom_call_target="tpu_custom_call" | custom-call | tf_op jit(solution)/shard_map/combine/pallas_call | solution.py:467
  72.2 2.7 %all-to-all-start.1 = ((bf16[32,64,128]{2,1,0:T(8,128)(2,1)}), bf16[32,64,128]{2,1,0:T(8,128)(2,1)S(1)}, u32[]{:S(2)}, u32[]{:S(2)}) async-start(bf16[32,64,128]{2,1,0:T(8,128)(2,1)} %get-tuple-element.35), calls=%async_computation.1 | async-start | bytes 1048576 | tf_op jit(solution)/shard_map/all_to_all | solution.py:489
  74.9 0.8 copy.24
  75.7 0.8 copy.25
  76.5 14.1 %all-to-all-done.1.in_ref = bf16[32,64,128]{2,1,0:T(8,128)(2,1)S(1)} async-done(((bf16[32,64,128]{2,1,0:T(8,128)(2,1)}), bf16[32,64,128]{2,1,0:T(8,128)(2,1)S(1)}, u32[]{:S(2)}, u32[]{:S(2)}) %all-to-all-start.1) | async-done | bytes 524320 | tf_op jit(solution)/shard_map/all_to_all | solution.py:489
  90.6 0.8 final.1
  (19 shorter events, 0.3 us)
Async XLA Ops:
  0.6 26.2 %copy-start.2 = (bf16[2,384,256]{2,1,0:T(8,128)(2,1)S(1)}, bf16[2,384,256]{2,1,0:T(8,128)(2,1)}, u32[]{:S(2)}) copy-start(bf16[2,384,256]{2,1,0:T(8,128)(2,1)} %param.10) | copy-start | bytes 1179652
  0.6 26.2 %copy-start.1 = (bf16[2,384,256]{2,1,0:T(8,128)(2,1)S(1)}, bf16[2,384,256]{2,1,0:T(8,128)(2,1)}, u32[]{:S(2)}) copy-start(bf16[2,384,256]{2,1,0:T(8,128)(2,1)} %param.7) | copy-start | bytes 1179652
  0.7 43.5 %collective-permute-start.7 = (bf16[192,4096]{1,0:T(8,128)(2,1)}, bf16[192,4096]{1,0:T(8,128)(2,1)}, u32[]{:S(2)}, u32[]{:S(2)}) collective-permute-start(bf16[192,4096]{1,0:T(8,128)(2,1)} %bitcast.15), channel_id=1, source_target_pairs={{0,2},{1,3},{2,0},{3,1},{4,6},{5,7},{6,4},{7,5},{8,10},{9,11},{10,... | collective-permute-start | bytes 4718600 | tf_op jit(solution)/shard_map/ppermute | solution.py:396
  4.8 11.7 %collective-permute-start = (bf16[768,128]{1,0:T(8,128)(2,1)S(1)}, bf16[768,128]{1,0:T(8,128)(2,1)S(1)}, u32[]{:S(2)}, u32[]{:S(2)}) collective-permute-start(bf16[768,128]{1,0:T(8,128)(2,1)S(1)} %bitcast.12), channel_id=1, source_target_pairs={{0,4},{4,0},{1,5},{5,1},{2,6},{6,2},{3,7},{7,3},{8,12},{12,8},{9,1... | collective-permute-start | bytes 589832 | tf_op jit(solution)/shard_map/ppermute | solution.py:378
  8.5 7.3 %collective-permute-start.3 = (s32[32]{0:T(128)S(1)}, s32[32]{0:T(128)S(1)}, u32[]{:S(2)}, u32[]{:S(2)}) collective-permute-start(s32[32]{0:T(128)S(1)} %reshape.74.table), channel_id=1, source_target_pairs={{24,0},{25,1},{26,2},{27,3},{28,4},{29,5},{30,6},{31,7}} | collective-permute-start | bytes 392 | tf_op jit(solution)/shard_map/ppermute | solution.py:391
  9.8 6.4 %collective-permute-start.2 = (s32[32]{0:T(128)S(1)}, s32[32]{0:T(128)S(1)}, u32[]{:S(2)}, u32[]{:S(2)}) collective-permute-start(s32[32]{0:T(128)S(1)} %reshape.74.table), channel_id=1, source_target_pairs={{16,0},{24,8},{17,1},{25,9},{18,2},{26,10},{19,3},{27,11},{20,4},{... | collective-permute-start | bytes 392 | tf_op jit(solution)/shard_map/ppermute | solution.py:391
  11.1 5.5 %collective-permute-start.1 = (s32[32]{0:T(128)S(1)}, s32[32]{0:T(128)S(1)}, u32[]{:S(2)}, u32[]{:S(2)}) collective-permute-start(s32[32]{0:T(128)S(1)} %reshape.74.table), channel_id=1, source_target_pairs={{8,0},{16,8},{24,16},{9,1},{17,9},{25,17},{10,2},{18,10},{26,18},{... | collective-permute-start | bytes 392 | tf_op jit(solution)/shard_map/ppermute | solution.py:391
  17.2 12.5 %collective-permute-start.4 = (bf16[512,128]{1,0:T(8,128)(2,1)S(1)}, bf16[512,128]{1,0:T(8,128)(2,1)S(1)}, u32[]{:S(2)}, u32[]{:S(2)}) collective-permute-start(bf16[512,128]{1,0:T(8,128)(2,1)S(1)} %get-tuple-element.25), channel_id=1, source_target_pairs={{0,8},{8,16},{16,24},{1,9},{9,17},{17,25},{2,10},{10,18},{18,26},{... | collective-permute-start | bytes 393224 | tf_op jit(solution)/shard_map/ppermute | solution.py:431
  21.2 8.5 %collective-permute-start.5 = (bf16[512,128]{1,0:T(8,128)(2,1)S(1)}, bf16[512,128]{1,0:T(8,128)(2,1)S(1)}, u32[]{:S(2)}, u32[]{:S(2)}) collective-permute-start(bf16[512,128]{1,0:T(8,128)(2,1)S(1)} %get-tuple-element.26), channel_id=1, source_target_pairs={{0,16},{8,24},{1,17},{9,25},{2,18},{10,26},{3,19},{11,27},{4,20},{... | collective-permute-start | bytes 393224 | tf_op jit(solution)/shard_map/ppermute | solution.py:431
  24.6 5.1 %collective-permute-start.6 = (bf16[512,128]{1,0:T(8,128)(2,1)S(1)}, bf16[512,128]{1,0:T(8,128)(2,1)S(1)}, u32[]{:S(2)}, u32[]{:S(2)}) collective-permute-start(bf16[512,128]{1,0:T(8,128)(2,1)S(1)} %get-tuple-element.27), channel_id=1, source_target_pairs={{0,24},{1,25},{2,26},{3,27},{4,28},{5,29},{6,30},{7,31}} | collective-permute-start | bytes 393224 | tf_op jit(solution)/shard_map/ppermute | solution.py:431
  25.9 41.3 %collective-permute-start.8 = (bf16[192,4096]{1,0:T(8,128)(2,1)}, bf16[192,4096]{1,0:T(8,128)(2,1)}, u32[]{:S(2)}, u32[]{:S(2)}) collective-permute-start(bf16[192,4096]{1,0:T(8,128)(2,1)} %bitcast.16), channel_id=1, source_target_pairs={{0,1},{1,0},{2,3},{3,2},{4,5},{5,4},{6,7},{7,6},{8,9},{9,8},{10,11... | collective-permute-start | bytes 4718600 | tf_op jit(solution)/shard_map/ppermute | solution.py:397
  29.7 37.5 %copy-start = (bf16[2,96,4096]{2,1,0:T(8,128)(2,1)S(1)}, bf16[2,96,4096]{2,1,0:T(8,128)(2,1)}, u32[]{:S(2)}) copy-start(bf16[2,96,4096]{2,1,0:T(8,128)(2,1)} %param.12) | copy-start | bytes 4718596
  44.1 23.1 %collective-permute-start.9 = (bf16[192,4096]{1,0:T(8,128)(2,1)}, bf16[192,4096]{1,0:T(8,128)(2,1)}, u32[]{:S(2)}, u32[]{:S(2)}) collective-permute-start(bf16[192,4096]{1,0:T(8,128)(2,1)} %collective-permute-done.7.refs_2_), channel_id=1, source_target_pairs={{0,1},{1,0},{2,3},{3,2},{4,5},{5,4},{6,7},{7,6},{8,9},{9,8},{10,11... | collective-permute-start | bytes 4718600 | tf_op jit(solution)/shard_map/ppermute | solution.py:461
  44.6 22.6 %all-to-all-start = ((bf16[8,272,128]{2,1,0:T(8,128)(2,1)}), bf16[8,272,128]{2,1,0:T(8,128)(2,1)S(1)}, u32[]{:S(2)}, u32[]{:S(2)}) async-start(bf16[8,272,128]{2,1,0:T(8,128)(2,1)} %get-tuple-element.31), calls=%async_computation | async-start | bytes 1114112 | tf_op jit(solution)/shard_map/all_to_all | solution.py:459
  72.2 18.4 %all-to-all-start.1 = ((bf16[32,64,128]{2,1,0:T(8,128)(2,1)}), bf16[32,64,128]{2,1,0:T(8,128)(2,1)S(1)}, u32[]{:S(2)}, u32[]{:S(2)}) async-start(bf16[32,64,128]{2,1,0:T(8,128)(2,1)} %get-tuple-element.35), calls=%async_computation.1 | async-start | bytes 1048576 | tf_op jit(solution)/shard_map/all_to_all | solution.py:489
where the time goes:
time: 91.9 us; the launch traced here: 91.4 us
  waiting for transfers between devices  34.1 us (37%)
  starting transfers between devices  27.2 us (30%)
  Pallas kernels  23.6 us (26%)
  local copies, waits for them, and re-layouts  3.03 us (3%)
  other arithmetic  2.62 us (3%)
    all_to_all x1, waiting for transfers between devices, on_device(): lax.all_to_all(attended[2], KV, split_axis=0, concat_axis=0, tiled=True)  15.8 us
    pallas_call x1, Pallas kernels, on_device(): pl.pallas_call(functools.partial(attend_kernel, n, nblk, bpd, heads, hd,...  14.4 us
    all_to_all x1, waiting for transfers between devices, on_device(): lax.all_to_all(partial, KV + ('tp',), split_axis=0, concat_axis=0, tiled=...  14.1 us
    ppermute x3, starting transfers between devices, on_device(): perm(packed[d - 1], 'hi', [(k, k + d) for k in range(pairs - d)])  8.67 us
    all_to_all x1, starting transfers between devices, on_device(): lax.all_to_all(attended[2], KV, split_axis=0, concat_axis=0, tiled=True)  6.72 us
    pallas_call x1, Pallas kernels, on_device(): pl.pallas_call(functools.partial(combine_kernel, n, seqs, bpd, hd, parts)...  5.04 us
    ppermute x3, waiting for transfers between devices, on_device(): perm(table, 'hi', [(k, k - d) for k in range(d, pairs)])  4.15 us
    ppermute x3, starting transfers between devices, on_device(): perm(table, 'hi', [(k, k - d) for k in range(d, pairs)])  3.88 us
  transfers between devices with their start and end apart: 12, of which 5 were waited for; matrix products, arithmetic and copies ran while one was open for 6% of the time, Pallas kernels for 19%

commit v1 on v0

--- a/solution.py
+++ b/solution.py
@@ -34,38 +34,72 @@
     return pl.BlockSpec(memory_space=SMEM)
 
 
+def front_kernel(n, seqs, bpd, ids_ref, key_ref, value_ref, kv_ref, table_ref):
+    tok = key_ref.shape[2]
+    for s in range(seqs):
+        both = jnp.concatenate([key_ref[s], value_ref[s]], axis=0).astype(F32)
+        kv_ref[s * tok : (s + 1) * tok, :] = both.T.astype(BF)
+    lane = lax.broadcasted_iota(jnp.int32, table_ref.shape, 1)
+    table = jnp.zeros(table_ref.shape, jnp.int32)
+    for s in range(seqs):
+        c = ids_ref[s, :, 0, :]
+        h = lax.shift_right_logical(c * -(-(1 << 20) // bpd), 20)
+        w = c - h * bpd
+        for k in range(n):
+            low = jnp.min(jnp.where(h == k, w, bpd - 1).astype(F32), keepdims=True)
+            high = jnp.max(jnp.where(h == k, w, 0).astype(F32), keepdims=True)
+            table = jnp.where(lane == k * seqs + s, low.astype(jnp.int32), table)
+            table = jnp.where(lane == (n + k) * seqs + s, high.astype(jnp.int32), table)
+    table_ref[...] = table
+
+
 def prep_kernel(
-    n, bpd, heads, hd, scale, ids, table, own_ref, q_ref, g_ref, gate_ref, r_ref, kv_loc, acc_loc
+    n,
+    seqs,
+    bpd,
+    heads,
+    hd,
+    scale,
+    table,
+    own_ref,
+    ids,
+    gate_ref,
+    q_ref,
+    g_ref,
+    r_ref,
+    kv_loc,
+    acc_loc,
+    gate_buf,
 ):
     width = 2 * hd
     rows = heads * BLK
-    low = lax.broadcasted_iota(jnp.int32, (BLK, width), 1) < hd
+    tok = bpd * BLK
+    for s in range(seqs):
+        gate_buf[s * tok : (s + 1) * tok, :] = jax.nn.sigmoid(gate_ref[s]).T
+    front = lax.broadcasted_iota(jnp.int32, (BLK, width), 1) < hd
 
     def step(i, carry):
         at = pl.ds(pl.multiple_of(i * BLK, BLK), BLK)
-        gates = jax.nn.sigmoid(gate_ref[at, :])
+        gates = gate_buf[at, :]
         for pair in range(heads // 2):
             q = q_ref[at, pair * width : (pair + 1) * width].astype(F32) * scale
             g = g_ref[at, pair * width : (pair + 1) * width].astype(F32)
-            gv = jnp.where(low, gates[:, 2 * pair : 2 * pair + 1], gates[:, 2 * pair + 1 : 2 * pair + 2])
+            gv = jnp.where(front, gates[:, 2 * pair : 2 * pair + 1], gates[:, 2 * pair + 1 : 2 * pair + 2])
             g = g * gv
             qr = pltpu.roll(q, hd, 1)
             gr = pltpu.roll(g, hd, 1)
             zero = jnp.zeros_like(q)
             base = 2 * pair * BLK
-            r_ref[i, base : base + BLK, :] = jnp.where(low, q, zero).astype(BF)
-            r_ref[i, base + BLK : base + 2 * BLK, :] = jnp.where(low, qr, zero).astype(BF)
-            r_ref[i, rows + base : rows + base + BLK, :] = jnp.where(low, zero, gr).astype(BF)
-            r_ref[i, rows + base + BLK : rows + base + 2 * BLK, :] = jnp.where(low, zero, g).astype(BF)
+            r_ref[i, base : base + BLK, :] = jnp.where(front, q, zero).astype(BF)
+            r_ref[i, base + BLK : base + 2 * BLK, :] = jnp.where(front, qr, zero).astype(BF)
+            r_ref[i, rows + base : rows + base + BLK, :] = jnp.where(front, zero, gr).astype(BF)
+            r_ref[i, rows + base + BLK : rows + base + 2 * BLK, :] = jnp.where(front, zero, g).astype(BF)
         return carry
 
-    nblk = q_ref.shape[0] // BLK
-    lax.fori_loop(0, nblk, step, 0)
-
-    seqs = nblk // bpd
+    nblk = seqs * bpd
     own = own_ref[0]
     dummy = nblk + n * seqs * MOST
-    named = ids[...]
+    named = jnp.concatenate([ids[s, :, 0, :] for s in range(seqs)], axis=0)
     row = lax.broadcasted_iota(jnp.int32, named.shape, 0)
     start = lax.broadcasted_iota(jnp.int32, named.shape, 1) == 0
     s = jnp.zeros_like(row)
@@ -77,9 +111,9 @@
     w = c - h * bpd
     low = jnp.zeros_like(c)
     for k in range(n):
-        here = jnp.full_like(c, table[k * seqs])
+        here = jnp.full_like(c, table[0, k * seqs])
         for q in range(1, seqs):
-            here = jnp.where(s == q, table[k * seqs + q], here)
+            here = jnp.where(s == q, table[0, k * seqs + q], here)
         low = jnp.where(h == k, here, low)
     slot = (w != low).astype(jnp.int32)
     own_z = lax.shift_right_logical(own, 1)
@@ -91,6 +125,8 @@
     kv_loc[...] = jnp.where(future, 0, jnp.where(h_z == own_z, near, far))
     remote = nblk + (h * seqs + s) * MOST + slot
     acc_loc[...] = jnp.where(future, dummy, jnp.where(h == own, home, remote))
+
+    lax.fori_loop(0, nblk, step, 0)
 
 
 def pack_kernel(seqs, bpd, n, shifts, *refs):
@@ -108,7 +144,7 @@
             for yh in range(2):
                 for m in range(MOST):
                     slot = (s * 2 + yh) * MOST + m
-                    lab = tables[d][m * n * seqs + (own - side + yh) * seqs + s]
+                    lab = tables[d][0, m * n * seqs + (own - side + yh) * seqs + s]
                     at = ((side ^ yh) * seqs + s) * bpd + lab
                     src = pl.multiple_of(at * BLK, BLK)
                     outs[d][slot * BLK : (slot + 1) * BLK, :] = both[pl.ds(src, BLK), :]
@@ -286,7 +322,7 @@
         out_ref[h, 0 : slots * BLK, :] = acc[lo : lo + slots * BLK, :].astype(BF)
         mark = jnp.zeros((LABEL_ROWS, width), F32)
         for k in range(slots):
-            lab = table[(k % MOST) * n * seqs + h * seqs + k // MOST]
+            lab = table[0, (k % MOST) * n * seqs + h * seqs + k // MOST]
             mark = jnp.where(lane == k, lab.astype(F32), mark)
         out_ref[h, slots * BLK : slots * BLK + LABEL_ROWS, :] = mark.astype(BF)
 
@@ -294,16 +330,19 @@
 def combine_kernel(n, seqs, bpd, hd, parts, quarter, own_ref, msgs, *refs):
     sources = refs[:parts]
     kg_ref, vg_ref, out_ref, total, vbuf, pieces, sems = refs[parts:]
-    cut = sources[0].shape[0] // CUTS
+    cut = sources[0].shape[1] // CUTS
     copies = [
-        pltpu.make_async_copy(
-            sources[j].at[pl.ds(q * cut, cut)], pieces.at[j, pl.ds(q * cut, cut)], sems.at[j, q]
-        )
+        [
+            pltpu.make_async_copy(
+                sources[j].at[:, pl.ds(q * cut, cut)], pieces.at[j, :, pl.ds(q * cut, cut)], sems.at[j, q]
+            )
+            for j in range(parts)
+        ]
         for q in range(CUTS)
-        for j in range(parts)
     ]
-    for copy in copies:
-        copy.start()
+    for group in copies:
+        for copy in group:
+            copy.start()
     slots = seqs * MOST
     total[...] = own_ref[...]
     for d in range(n):
@@ -331,9 +370,10 @@
         ]
         turned.append(jnp.concatenate(v, axis=0).T.astype(BF))
     lanes = out_ref.shape[2]
-    for copy in copies:
-        copy.wait()
     for i in range(out_ref.shape[0] // 2):
+        if (2 * i * lanes) % cut == 0:
+            for copy in copies[2 * i * lanes // cut]:
+                copy.wait()
         acc = jnp.zeros((hd, 2 * lanes), F32)
         for j in range(parts):
             x = pieces[j, :, 2 * i * lanes : 2 * (i + 1) * lanes]
@@ -374,19 +414,22 @@
     width = 2 * hd
 
     perm = lax.ppermute
-    kv = jnp.concatenate([key_states, value_states], axis=-1).reshape(nblk * BLK, width)
+    own_at = own.reshape(1)
+    lanes = -(-MOST * n * seqs // 128) * 128
+    kv, table = pl.pallas_call(
+        functools.partial(front_kernel, n, seqs, bpd),
+        out_shape=[
+            jax.ShapeDtypeStruct((seqs * tok, width), BF),
+            jax.ShapeDtypeStruct((1, lanes), jnp.int32),
+        ],
+        in_specs=[vspec()] * 3,
+        out_specs=[vspec()] * 2,
+        compiler_params=grant(3),
+        name="front",
+    )(chosen, key_states.transpose(0, 2, 1), value_states.transpose(0, 2, 1))
+    perm = lax.ppermute
     partner = perm(kv, "lo", [(0, 1), (1, 0)])
 
-    kv, chosen = lax.optimization_barrier((kv, chosen))
-    ids = chosen[:, :, 0, :]
-    flat = ids.reshape(seqs, bpd * picks)
-    holder = (flat // bpd)[None]
-    within = (flat % bpd)[None]
-    hit = holder == jnp.arange(n, dtype=jnp.int32)[:, None, None]
-    low = jnp.min(jnp.where(hit, within, bpd - 1), axis=-1)
-    high = jnp.max(jnp.where(hit, within, 0), axis=-1)
-    table = jnp.stack([low, high]).reshape(MOST * n * seqs)
-    own_at = own.reshape(1)
     asked = [
         perm(table, "hi", [(k, k - d) for k in range(d, pairs)]) for d in range(1, pairs)
     ]
@@ -397,24 +440,25 @@
     piece1 = perm(mine, "tp", tp_xor(1))
 
     prepare = pl.pallas_call(
-        functools.partial(prep_kernel, n, bpd, heads, hd, scale),
+        functools.partial(prep_kernel, n, seqs, bpd, heads, hd, scale),
         out_shape=[
             jax.ShapeDtypeStruct((nblk, 2 * heads * BLK, width), BF),
             jax.ShapeDtypeStruct((nblk, picks), jnp.int32),
             jax.ShapeDtypeStruct((nblk, picks), jnp.int32),
         ],
-        in_specs=[vspec()] + [sspec()] * 2 + [vspec()] * 3,
+        in_specs=[sspec()] * 2 + [vspec()] * 4,
         out_specs=[vspec()] * 3,
+        scratch_shapes=[VMEM((seqs * tok, heads), F32)],
         compiler_params=grant(3),
         name="prep",
     )
     r, kv_loc, acc_loc = prepare(
-        ids.reshape(nblk, picks),
         table,
         own_at,
+        chosen,
+        gate_logits.transpose(0, 2, 1),
         queries.reshape(seqs * tok, row_width),
         cotangent.reshape(seqs * tok, row_width),
-        gate_logits.reshape(seqs * tok, heads),
     )
 
     zrows = slots * 2 * BLK

time: 91.9 us -> 90.4 us (0.984)
  local copies, waits for them, and re-layouts: 3.03 us -> 7.41 us
  starting transfers between devices: 27.2 us -> 24.5 us
  other arithmetic: 2.62 us -> 0 us
    unnamed x9 -> x18, local copies, waits for them, and re-layouts: 2.44 us -> 7.41 us
    all_to_all x1, starting transfers between devices: 6.72 us -> 4.1 us  [on_device(): lax.all_to_all(attended[2], KV, split_axis=0, concat_axis=0, tiled=True)]
    pallas_call x1, Pallas kernels: 5.04 us -> 3.89 us  [on_device(): pl.pallas_call(functools.partial(combine_kernel, n, seqs, bpd, hd, parts)...]
    concatenate x1 -> x0, other arithmetic: 0.96 us -> none  [on_device(): jnp.concatenate([key_states, value_states], axis=-1)]
    pallas_call x1 -> x2, Pallas kernels: 2.78 us -> 3.19 us  [the longest x1 2.93 us: on_device(): prepare(table, own_at, chosen, gate_logits.transpose(0, 2, 1), queries.re...]
  transfers between devices with their start and end apart: 12 -> 12, of which waited for: 5 -> 5; matrix products, arithmetic and copies ran while one was open for 6% -> 2% of each run, Pallas kernels for 19% -> 20%
where the time goes in v1:
time: 90.4 us; the launch traced here: 89.7 us
  waiting for transfers between devices  34.1 us (38%)
  starting transfers between devices  24.5 us (27%)
  Pallas kernels  22.9 us (25%)
  local copies, waits for them, and re-layouts  7.41 us (8%)
    all_to_all x1, waiting for transfers between devices, on_device(): lax.all_to_all(attended[2], KV, split_axis=0, concat_axis=0, tiled=True)  15.8 us
    pallas_call x1, Pallas kernels, on_device(): pl.pallas_call(functools.partial(attend_kernel, n, nblk, bpd, heads, hd,...  14.4 us
    all_to_all x1, waiting for transfers between devices, on_device(): lax.all_to_all(partial, KV + ('tp',), split_axis=0, concat_axis=0, tiled=...  14.1 us
    ppermute x3, starting transfers between devices, on_device(): perm(packed[d - 1], 'hi', [(k, k + d) for k in range(pairs - d)])  8.67 us
    unnamed x18, local copies, waits for them, and re-layouts  7.41 us
    ppermute x3, waiting for transfers between devices, on_device(): perm(table, 'hi', [(k, k - d) for k in range(d, pairs)])  4.15 us
    all_to_all x1, starting transfers between devices, on_device(): lax.all_to_all(attended[2], KV, split_axis=0, concat_axis=0, tiled=True)  4.1 us
    pallas_call x1, Pallas kernels, on_device(): pl.pallas_call(functools.partial(combine_kernel, n, seqs, bpd, hd, parts)...  3.89 us
  transfers between devices with their start and end apart: 12, of which 5 were waited for; matrix products, arithmetic and copies ran while one was open for 2% of the time, Pallas kernels for 20%

profile of v1, /device:TPU:0, one launch (start us, length us, event | category | flops | bytes accessed | tf_op | source)
XLA Modules:
  0.0 89.7 jit_solution(12700663507904739191)
XLA Ops:
  0.6 3.0 %collective-permute-start.7 = (bf16[192,4096]{1,0:T(8,128)(2,1)}, bf16[192,4096]{1,0:T(8,128)(2,1)}, u32[]{:S(2)}, u32[]{:S(2)}) collective-permute-start(bf16[192,4096]{1,0:T(8,128)(2,1)} %bitcast.11), channel_id=1, source_target_pairs={{0,2},{1,3},{2,0},{3,1},{4,6},{5,7},{6,4},{7,5},{8,10},{9,11},{10,... | collective-permute-start | bytes 4718600 | tf_op jit(solution)/shard_map/ppermute | solution.py:439
  3.7 0.9 copy-done.3
  4.6 0.9 copy-done.4
  5.5 0.7 copy-done.5
  6.1 0.3 front.1
  6.4 1.6 %collective-permute-start = (bf16[768,128]{1,0:T(8,128)(2,1)S(1)}, bf16[768,128]{1,0:T(8,128)(2,1)S(1)}, u32[]{:S(2)}, u32[]{:S(2)}) collective-permute-start(bf16[768,128]{1,0:T(8,128)(2,1)S(1)} %get-tuple-element.24.refs_4_.kv_ref), channel_id=1, source_target_pairs={{0,4},{4,0},{1,5},{5,1},{2,6},{6,2},{3,7},{7,3},{8,12},{12,8},{9,1... | collective-permute-start | bytes 589832 | tf_op jit(solution)/shard_map/ppermute | solution.py:431
  8.0 1.3 %collective-permute-start.3 = (s32[1,128]{1,0:T(1,128)S(1)}, s32[1,128]{1,0:T(1,128)S(1)}, u32[]{:S(2)}, u32[]{:S(2)}) collective-permute-start(s32[1,128]{1,0:T(1,128)S(1)} %get-tuple-element.20.table), channel_id=1, source_target_pairs={{24,0},{25,1},{26,2},{27,3},{28,4},{29,5},{30,6},{31,7}} | collective-permute-start | bytes 1544 | tf_op jit(solution)/shard_map/ppermute | solution.py:434
  9.3 1.3 %collective-permute-start.2 = (s32[1,128]{1,0:T(1,128)S(1)}, s32[1,128]{1,0:T(1,128)S(1)}, u32[]{:S(2)}, u32[]{:S(2)}) collective-permute-start(s32[1,128]{1,0:T(1,128)S(1)} %get-tuple-element.20.table), channel_id=1, source_target_pairs={{16,0},{24,8},{17,1},{25,9},{18,2},{26,10},{19,3},{27,11},{20,4},{... | collective-permute-start | bytes 1544 | tf_op jit(solution)/shard_map/ppermute | solution.py:434
  10.6 1.3 %collective-permute-start.1 = (s32[1,128]{1,0:T(1,128)S(1)}, s32[1,128]{1,0:T(1,128)S(1)}, u32[]{:S(2)}, u32[]{:S(2)}) collective-permute-start(s32[1,128]{1,0:T(1,128)S(1)} %get-tuple-element.20.table), channel_id=1, source_target_pairs={{8,0},{16,8},{24,16},{9,1},{17,9},{25,17},{10,2},{18,10},{26,18},{... | collective-permute-start | bytes 1544 | tf_op jit(solution)/shard_map/ppermute | solution.py:434
  11.9 3.4 %collective-permute-done.3.refs_2_ = s32[1,128]{1,0:T(1,128)S(1)} collective-permute-done((s32[1,128]{1,0:T(1,128)S(1)}, s32[1,128]{1,0:T(1,128)S(1)}, u32[]{:S(2)}, u32[]{:S(2)}) %collective-permute-start.3) | collective-permute-done | bytes 544 | tf_op jit(solution)/shard_map/ppermute | solution.py:434
  15.3 0.4 collective-permute-done.2.refs_1_
  15.7 0.4 collective-permute-done.1.refs_0_
  16.1 0.6 pack.1
  16.7 4.0 %collective-permute-start.4 = (bf16[512,128]{1,0:T(8,128)(2,1)S(1)}, bf16[512,128]{1,0:T(8,128)(2,1)S(1)}, u32[]{:S(2)}, u32[]{:S(2)}) collective-permute-start(bf16[512,128]{1,0:T(8,128)(2,1)S(1)} %get-tuple-element.25), channel_id=1, source_target_pairs={{0,8},{8,16},{16,24},{1,9},{9,17},{17,25},{2,10},{10,18},{18,26},{... | collective-permute-start | bytes 393224 | tf_op jit(solution)/shard_map/ppermute | solution.py:475
  20.7 3.4 %collective-permute-start.5 = (bf16[512,128]{1,0:T(8,128)(2,1)S(1)}, bf16[512,128]{1,0:T(8,128)(2,1)S(1)}, u32[]{:S(2)}, u32[]{:S(2)}) collective-permute-start(bf16[512,128]{1,0:T(8,128)(2,1)S(1)} %get-tuple-element.26), channel_id=1, source_target_pairs={{0,16},{8,24},{1,17},{9,25},{2,18},{10,26},{3,19},{11,27},{4,20},{... | collective-permute-start | bytes 393224 | tf_op jit(solution)/shard_map/ppermute | solution.py:475
  24.1 1.3 %collective-permute-start.6 = (bf16[512,128]{1,0:T(8,128)(2,1)S(1)}, bf16[512,128]{1,0:T(8,128)(2,1)S(1)}, u32[]{:S(2)}, u32[]{:S(2)}) collective-permute-start(bf16[512,128]{1,0:T(8,128)(2,1)S(1)} %get-tuple-element.27), channel_id=1, source_target_pairs={{0,24},{1,25},{2,26},{3,27},{4,28},{5,29},{6,30},{7,31}} | collective-permute-start | bytes 393224 | tf_op jit(solution)/shard_map/ppermute | solution.py:475
  25.4 0.1 collective-permute-start.8
  25.5 1.0 %copy-done.1 = bf16[2,384,256]{2,1,0:T(8,128)(2,1)S(1)} copy-done((bf16[2,384,256]{2,1,0:T(8,128)(2,1)S(1)}, bf16[2,384,256]{2,1,0:T(8,128)(2,1)}, u32[]{:S(2)}) %copy-start.1) | copy-done | bytes 393240
  26.4 1.0 %copy-done.2 = bf16[2,384,256]{2,1,0:T(8,128)(2,1)S(1)} copy-done((bf16[2,384,256]{2,1,0:T(8,128)(2,1)S(1)}, bf16[2,384,256]{2,1,0:T(8,128)(2,1)}, u32[]{:S(2)}) %copy-start.2) | copy-done | bytes 393240
  27.4 0.7 copy-done.6
  28.1 0.7 copy-done.7
  28.8 2.9 %prep.1 = (bf16[12,512,128]{2,1,0:T(8,128)(2,1)S(1)}, s32[12,16]{1,0:T(8,128)S(1)}, s32[12,16]{1,0:T(8,128)S(1)}) custom-call(s32[1,128]{1,0:T(1,128)S(1)} %get-tuple-element.20.table, s32[1]{0:T(128)} %bitcast.2.own_ref.refs_3_, s32[2,6,1,16]{3,2,1,0:T(1,128)S(1)} %copy-done.6, f32[2,4,384]{2,1,0:T(4,128)S(1)} %bitcast.20, bf16[768,256]{1,0:T(8,128)(2,1)S(1)} %bitcast.14, ...), custom_call_target="tpu_custom_call" | custom-call | tf_op jit(solution)/shard_map/prep/pallas_call | solution.py:455
  31.8 14.4 %attend.1 = (bf16[768,256]{1,0:T(8,128)(2,1)}, f32[768,128]{1,0:T(8,128)S(1)}, bf16[8,272,128]{2,1,0:T(8,128)(2,1)}) custom-call(s32[12,16]{1,0:T(8,128)S(1)} %get-tuple-element.21.kv_loc, s32[12,16]{1,0:T(8,128)S(1)} %get-tuple-element.22.acc_loc, s32[1,128]{1,0:T(1,128)S(1)} %get-tuple-element.20.table, bf16[12,512,128]{2,1,0:T(8,128)(2,1)S(1)} %get-tuple-element.23.r_ref, ...), custom_call_target="tpu_custom_call" | custom-call | tf_op jit(solution)/shard_map/attend/pallas_call | solution.py:482
  46.2 0.5 collective-permute-start.9
  46.7 4.1 %all-to-all-start = ((bf16[8,272,128]{2,1,0:T(8,128)(2,1)}), bf16[8,272,128]{2,1,0:T(8,128)(2,1)S(1)}, u32[]{:S(2)}, u32[]{:S(2)}) async-start(bf16[8,272,128]{2,1,0:T(8,128)(2,1)} %get-tuple-element.31), calls=%async_computation | async-start | bytes 1114112 | tf_op jit(solution)/shard_map/all_to_all | solution.py:503
  50.8 15.8 %all-to-all-done.msgs = bf16[8,272,128]{2,1,0:T(8,128)(2,1)S(1)} async-done(((bf16[8,272,128]{2,1,0:T(8,128)(2,1)}), bf16[8,272,128]{2,1,0:T(8,128)(2,1)S(1)}, u32[]{:S(2)}, u32[]{:S(2)}) %all-to-all-start) | async-done | bytes 557088 | tf_op jit(solution)/shard_map/all_to_all | solution.py:503
  66.7 3.9 %combine.1 = (bf16[768,64]{1,0:T(8,128)(2,1)S(1)}, bf16[768,64]{1,0:T(8,128)(2,1)S(1)}, bf16[32,64,128]{2,1,0:T(8,128)(2,1)}) custom-call(s32[1]{0:T(128)} %bitcast.7.quarter, f32[768,128]{1,0:T(8,128)S(1)} %get-tuple-element.30.own_ref, bf16[8,272,128]{2,1,0:T(8,128)(2,1)S(1)} %all-to-all-done.msgs, bf16[192,4096]{1,0:T(8,128)(2,1)S(1)} %bitcast.13, ...), custom_call_target="tpu_custom_call" | custom-call | tf_op jit(solution)/shard_map/combine/pallas_call | solution.py:511
  70.5 2.7 %all-to-all-start.1 = ((bf16[32,64,128]{2,1,0:T(8,128)(2,1)}), bf16[32,64,128]{2,1,0:T(8,128)(2,1)S(1)}, u32[]{:S(2)}, u32[]{:S(2)}) async-start(bf16[32,64,128]{2,1,0:T(8,128)(2,1)} %get-tuple-element.35), calls=%async_computation.1 | async-start | bytes 1048576 | tf_op jit(solution)/shard_map/all_to_all | solution.py:533
  73.3 0.8 copy.11
  74.1 0.8 copy.12
  74.8 14.1 %all-to-all-done.1.in_ref = bf16[32,64,128]{2,1,0:T(8,128)(2,1)S(1)} async-done(((bf16[32,64,128]{2,1,0:T(8,128)(2,1)}), bf16[32,64,128]{2,1,0:T(8,128)(2,1)S(1)}, u32[]{:S(2)}, u32[]{:S(2)}) %all-to-all-start.1) | async-done | bytes 524320 | tf_op jit(solution)/shard_map/all_to_all | solution.py:533
  88.9 0.8 final.1
  (16 shorter events, 0.0 us)
Async XLA Ops:
  0.6 45.6 %collective-permute-start.7 = (bf16[192,4096]{1,0:T(8,128)(2,1)}, bf16[192,4096]{1,0:T(8,128)(2,1)}, u32[]{:S(2)}, u32[]{:S(2)}) collective-permute-start(bf16[192,4096]{1,0:T(8,128)(2,1)} %bitcast.11), channel_id=1, source_target_pairs={{0,2},{1,3},{2,0},{3,1},{4,6},{5,7},{6,4},{7,5},{8,10},{9,11},{10,... | collective-permute-start | bytes 4718600 | tf_op jit(solution)/shard_map/ppermute | solution.py:439
  3.7 0.9 copy-start.3
  4.6 0.9 copy-start.4
  5.4 0.7 copy-start.5
  6.4 9.6 %collective-permute-start = (bf16[768,128]{1,0:T(8,128)(2,1)S(1)}, bf16[768,128]{1,0:T(8,128)(2,1)S(1)}, u32[]{:S(2)}, u32[]{:S(2)}) collective-permute-start(bf16[768,128]{1,0:T(8,128)(2,1)S(1)} %get-tuple-element.24.refs_4_.kv_ref), channel_id=1, source_target_pairs={{0,4},{4,0},{1,5},{5,1},{2,6},{6,2},{3,7},{7,3},{8,12},{12,8},{9,1... | collective-permute-start | bytes 589832 | tf_op jit(solution)/shard_map/ppermute | solution.py:431
  8.0 7.2 %collective-permute-start.3 = (s32[1,128]{1,0:T(1,128)S(1)}, s32[1,128]{1,0:T(1,128)S(1)}, u32[]{:S(2)}, u32[]{:S(2)}) collective-permute-start(s32[1,128]{1,0:T(1,128)S(1)} %get-tuple-element.20.table), channel_id=1, source_target_pairs={{24,0},{25,1},{26,2},{27,3},{28,4},{29,5},{30,6},{31,7}} | collective-permute-start | bytes 1544 | tf_op jit(solution)/shard_map/ppermute | solution.py:434
  9.3 6.4 %collective-permute-start.2 = (s32[1,128]{1,0:T(1,128)S(1)}, s32[1,128]{1,0:T(1,128)S(1)}, u32[]{:S(2)}, u32[]{:S(2)}) collective-permute-start(s32[1,128]{1,0:T(1,128)S(1)} %get-tuple-element.20.table), channel_id=1, source_target_pairs={{16,0},{24,8},{17,1},{25,9},{18,2},{26,10},{19,3},{27,11},{20,4},{... | collective-permute-start | bytes 1544 | tf_op jit(solution)/shard_map/ppermute | solution.py:434
  10.6 5.5 %collective-permute-start.1 = (s32[1,128]{1,0:T(1,128)S(1)}, s32[1,128]{1,0:T(1,128)S(1)}, u32[]{:S(2)}, u32[]{:S(2)}) collective-permute-start(s32[1,128]{1,0:T(1,128)S(1)} %get-tuple-element.20.table), channel_id=1, source_target_pairs={{8,0},{16,8},{24,16},{9,1},{17,9},{25,17},{10,2},{18,10},{26,18},{... | collective-permute-start | bytes 1544 | tf_op jit(solution)/shard_map/ppermute | solution.py:434
  16.7 15.1 %collective-permute-start.4 = (bf16[512,128]{1,0:T(8,128)(2,1)S(1)}, bf16[512,128]{1,0:T(8,128)(2,1)S(1)}, u32[]{:S(2)}, u32[]{:S(2)}) collective-permute-start(bf16[512,128]{1,0:T(8,128)(2,1)S(1)} %get-tuple-element.25), channel_id=1, source_target_pairs={{0,8},{8,16},{16,24},{1,9},{9,17},{17,25},{2,10},{10,18},{18,26},{... | collective-permute-start | bytes 393224 | tf_op jit(solution)/shard_map/ppermute | solution.py:475
  20.7 11.1 %collective-permute-start.5 = (bf16[512,128]{1,0:T(8,128)(2,1)S(1)}, bf16[512,128]{1,0:T(8,128)(2,1)S(1)}, u32[]{:S(2)}, u32[]{:S(2)}) collective-permute-start(bf16[512,128]{1,0:T(8,128)(2,1)S(1)} %get-tuple-element.26), channel_id=1, source_target_pairs={{0,16},{8,24},{1,17},{9,25},{2,18},{10,26},{3,19},{11,27},{4,20},{... | collective-permute-start | bytes 393224 | tf_op jit(solution)/shard_map/ppermute | solution.py:475
  24.1 7.7 %collective-permute-start.6 = (bf16[512,128]{1,0:T(8,128)(2,1)S(1)}, bf16[512,128]{1,0:T(8,128)(2,1)S(1)}, u32[]{:S(2)}, u32[]{:S(2)}) collective-permute-start(bf16[512,128]{1,0:T(8,128)(2,1)S(1)} %get-tuple-element.27), channel_id=1, source_target_pairs={{0,24},{1,25},{2,26},{3,27},{4,28},{5,29},{6,30},{7,31}} | collective-permute-start | bytes 393224 | tf_op jit(solution)/shard_map/ppermute | solution.py:475
  25.4 41.3 %collective-permute-start.8 = (bf16[192,4096]{1,0:T(8,128)(2,1)}, bf16[192,4096]{1,0:T(8,128)(2,1)}, u32[]{:S(2)}, u32[]{:S(2)}) collective-permute-start(bf16[192,4096]{1,0:T(8,128)(2,1)} %bitcast.12), channel_id=1, source_target_pairs={{0,1},{1,0},{2,3},{3,2},{4,5},{5,4},{6,7},{7,6},{8,9},{9,8},{10,11... | collective-permute-start | bytes 4718600 | tf_op jit(solution)/shard_map/ppermute | solution.py:440
  25.4 1.0 %copy-start.1 = (bf16[2,384,256]{2,1,0:T(8,128)(2,1)S(1)}, bf16[2,384,256]{2,1,0:T(8,128)(2,1)}, u32[]{:S(2)}) copy-start(bf16[2,384,256]{2,1,0:T(8,128)(2,1)} %param.7) | copy-start | bytes 1179652
  26.4 1.0 %copy-start.2 = (bf16[2,384,256]{2,1,0:T(8,128)(2,1)S(1)}, bf16[2,384,256]{2,1,0:T(8,128)(2,1)}, u32[]{:S(2)}) copy-start(bf16[2,384,256]{2,1,0:T(8,128)(2,1)} %param.10) | copy-start | bytes 1179652
  27.4 0.7 copy-start.6
  28.1 0.7 copy-start.7
  31.8 34.9 %copy-start = (bf16[2,96,4096]{2,1,0:T(8,128)(2,1)S(1)}, bf16[2,96,4096]{2,1,0:T(8,128)(2,1)}, u32[]{:S(2)}) copy-start(bf16[2,96,4096]{2,1,0:T(8,128)(2,1)} %param.12) | copy-start | bytes 4718596
  46.2 20.4 %collective-permute-start.9 = (bf16[192,4096]{1,0:T(8,128)(2,1)}, bf16[192,4096]{1,0:T(8,128)(2,1)}, u32[]{:S(2)}, u32[]{:S(2)}) collective-permute-start(bf16[192,4096]{1,0:T(8,128)(2,1)} %collective-permute-done.7.refs_2_), channel_id=1, source_target_pairs={{0,1},{1,0},{2,3},{3,2},{4,5},{5,4},{6,7},{7,6},{8,9},{9,8},{10,11... | collective-permute-start | bytes 4718600 | tf_op jit(solution)/shard_map/ppermute | solution.py:505
  46.7 19.9 %all-to-all-start = ((bf16[8,272,128]{2,1,0:T(8,128)(2,1)}), bf16[8,272,128]{2,1,0:T(8,128)(2,1)S(1)}, u32[]{:S(2)}, u32[]{:S(2)}) async-start(bf16[8,272,128]{2,1,0:T(8,128)(2,1)} %get-tuple-element.31), calls=%async_computation | async-start | bytes 1114112 | tf_op jit(solution)/shard_map/all_to_all | solution.py:503
  70.5 18.4 %all-to-all-start.1 = ((bf16[32,64,128]{2,1,0:T(8,128)(2,1)}), bf16[32,64,128]{2,1,0:T(8,128)(2,1)S(1)}, u32[]{:S(2)}, u32[]{:S(2)}) async-start(bf16[32,64,128]{2,1,0:T(8,128)(2,1)} %get-tuple-element.35), calls=%async_computation.1 | async-start | bytes 1048576 | tf_op jit(solution)/shard_map/all_to_all | solution.py:533
